TPU v7x, 32 devices: a whole 2x2x4 slice. The times are simulated.
32 devices in a mesh: ep: 4 (over y, x), tp: 8 (over z, core).
Axes of the slice: x: 2, y: 2, z: 4, core: 2. Of those that a mesh axis runs over, the one named last changes fastest.
Arguments:
- residual: bfloat16 [128, 2048], P('ep'), may hold values from -6 to 6
- mixer_gain: float32 [2048], replicated, may hold values from 0.1 to 1.9
- gate_proj: bfloat16 [2048, 2048], P('ep', 'tp'), may hold values from -0.125 to 0.125
- input_proj: bfloat16 [2048, 2048], P('ep', 'tp'), may hold values from -0.125 to 0.125
- write_proj: bfloat16 [2048, 2048], P('ep', 'tp'), may hold values from -0.125 to 0.125
- read_proj: bfloat16 [2048, 2048], P('ep', 'tp'), may hold values from -0.125 to 0.125
- step_proj: bfloat16 [2048, 32], replicated, may hold values from -0.125 to 0.125
- conv_weight: float32 [4, 3, 2048], replicated, may hold values from -3 to 3
- step_bias: float32 [32], replicated, may hold values from -4 to 0
- log_rate: float32 [32], replicated, may hold values from 0 to 2.5
- skip_gain: float32 [32], replicated, may hold values from -4 to 4
- group_gain: float32 [2048], replicated, may hold values from 0.1 to 1.9
- ssm_state: float32 [128, 32, 64, 128], P('ep', 'tp'), may hold values from -2 to 2
- conv_state: bfloat16 [128, 3, 3, 2048], P('ep', None, None, 'tp'), may hold values from -6 to 6
- out_proj: bfloat16 [2048, 2048], P('tp'), may hold values from -0.125 to 0.125
- ffn_gain: float32 [2048], replicated, may hold values from 0.1 to 1.9
- routes: int32 [128, 2], P('ep'), may hold values from 0 to 7, all different within a row; in each aligned block of 32 rows (0 to 31, 32 to 63, ...) at most 16 rows name the same one
- route_weight: float32 [128, 2], P('ep'), may hold values from 0.2 to 1
- expert_gate: bfloat16 [8, 2048, 2048], P('ep', None, 'tp'), may hold values from -0.125 to 0.125
- expert_up: bfloat16 [8, 2048, 2048], P('ep', None, 'tp'), may hold values from -0.125 to 0.125
- expert_down: bfloat16 [8, 2048, 2048], P('ep', 'tp'), may hold values from -0.125 to 0.125
- dense_gate: bfloat16 [2048, 2048], P(None, 'tp'), may hold values from -0.125 to 0.125
- dense_up: bfloat16 [2048, 2048], P(None, 'tp'), may hold values from -0.125 to 0.125
- dense_down: bfloat16 [2048, 2048], P('tp'), may hold values from -0.125 to 0.125
- blend_weight: bfloat16 [2048], replicated, may hold values from -0.125 to 0.125
Outputs:
- layer_out: bfloat16 [128, 2048], P('ep', 'tp')
- new_state: float32 [128, 32, 64, 128], P('ep', 'tp')
- new_conv: bfloat16 [128, 3, 3, 2048], P('ep', None, None, 'tp')
Inputs may be any that keep to these rules, and one draw needn't show every extreme that they name: `routes`: each row names 2 different experts. Within the 32 rows of one index of ep no expert is named by more than 16 rows, and in some such block some expert is named by exactly 16 rows.
All inputs are finite; a program needn't handle non-finite values.
Results may differ from a plain program's by a relative error of at most 0.015.
Values may be sent and summed in bfloat16 or wider, within the bound.
A program may use at most 128 MiB of HBM per device.

v0:
```python
import functools
import jax
import jax.numpy as jnp
from jax import lax
from jax.experimental import pallas as pl
from jax.experimental.pallas import tpu as pltpu
from jax.sharding import PartitionSpec as P

epsilon = 1e-06
F32 = jnp.float32
BF16 = jnp.bfloat16
MESH = pl.DeviceIdType.MESH
VM = pl.BlockSpec(memory_space=pltpu.VMEM)
HB = pl.BlockSpec(memory_space=pl.ANY)
GRANT = 67043328


def mm(a, b):
    return jnp.dot(a, b, preferred_element_type=F32)


def nt(a, b):
    return lax.dot_general(a, b, (((1,), (1,)), ((), ())), preferred_element_type=F32)


def silu(v):
    return v * jax.nn.sigmoid(v)


def proj_kernel(
    N, res_ref, gain_ref, wg, wx, wb, wc, step_ref, out_ref, raw_ref,
    w, nb, pieces, outb, inb, wsem, s1, r1, s2, r2,
):
    ep, tp = lax.axis_index("ep"), lax.axis_index("tp")
    R, D = res_ref.shape
    K = D // N
    W = wg.shape[1]
    loads = [pltpu.make_async_copy(src, w.at[i], wsem.at[i]) for i, src in enumerate((wg, wx, wb, wc))]
    for c in loads:
        c.start()
    bar = pltpu.get_barrier_semaphore()

    def greet(o, _):
        pl.semaphore_signal(bar, inc=1, device_id=(lax.rem(ep + o, N), tp), device_id_type=MESH)
        return 0

    lax.fori_loop(1, N, greet, 0)
    x = res_ref[...].astype(F32)
    normed = x * lax.rsqrt(jnp.mean(x * x, axis=-1, keepdims=True) + epsilon) * gain_ref[...]
    normed = normed.astype(BF16)
    for k in range(N):
        nb[k] = normed[:, k * K:(k + 1) * K]
    pl.semaphore_wait(bar, N - 1)

    def copy1(src_slot, dst_slot, peer, sem):
        return pltpu.make_async_remote_copy(
            src_ref=nb.at[src_slot], dst_ref=pieces.at[dst_slot], send_sem=s1.at[src_slot],
            recv_sem=r1.at[sem], device_id=(peer, tp), device_id_type=MESH)

    def send1(o, _):
        p = lax.rem(ep + o, N)
        copy1(p, ep, p, ep).start()
        return 0

    lax.fori_loop(1, N, send1, 0)
    raw_ref[...] = nt(normed, step_ref[...])
    for c in loads:
        c.wait()
    own = [mm(nb[ep], w[i]) for i in range(4)]

    def copy2(src_slot, dst_slot, peer, sem):
        return pltpu.make_async_remote_copy(
            src_ref=outb.at[src_slot], dst_ref=inb.at[dst_slot], send_sem=s2.at[src_slot],
            recv_sem=r2.at[sem], device_id=(peer, tp), device_id_type=MESH)

    def step(o, _):
        p = lax.rem(ep + o, N)
        copy1(p, p, p, p).wait_recv()
        a = pieces[p]
        for i in range(4):
            outb[p, :, i * W:(i + 1) * W] = mm(a, w[i]).astype(BF16)
        copy2(p, ep, p, ep).start()
        return 0

    lax.fori_loop(1, N, step, 0)
    total = jnp.concatenate(own, axis=1)
    for o in range(1, N):
        p = lax.rem(ep + o, N)
        copy2(p, p, p, p).wait_recv()
        total = total + inb[p].astype(F32)
    out_ref[...] = total.astype(BF16)

    def fin(o, _):
        p = lax.rem(ep + o, N)
        copy1(p, p, p, p).wait_send()
        copy2(p, p, p, p).wait_send()
        return 0

    lax.fori_loop(1, N, fin, 0)


def mixer_kernel(
    proj_ref, raw_ref, bias_ref, rate_ref, skip_ref, gain_ref, taps_ref, conv_ref, st_ref,
    ns_ref, nc_ref, out_ref, act, dec_rows,
):
    B, H, PD, S = st_ref.shape
    W = H * PD
    G = W // S
    tp = lax.axis_index("tp")
    own_cols = pl.ds(pl.multiple_of(tp * W, W), W)
    step_id = pl.program_id(0)

    @pl.when(step_id == 0)
    def _():
        heads = raw_ref.shape[1]
        R = raw_ref.shape[0]
        kept = conv_ref.shape[0]
        channels = []
        for c in range(3):
            newest = proj_ref[:, (c + 1) * W:(c + 2) * W]
            taps = taps_ref[c, :, own_cols]
            total = newest.astype(F32) * taps[kept:kept + 1]
            for k in range(kept):
                total = total + conv_ref[k, c].astype(F32) * taps[k:k + 1]
            for k in range(kept - 1):
                nc_ref[k, c] = conv_ref[k + 1, c]
            nc_ref[kept - 1, c] = newest
            channels.append(silu(total))
        size = jax.nn.softplus(raw_ref[...] + bias_ref[...])
        decay = jnp.exp(-jnp.exp(rate_ref[...]) * size)
        table = jnp.concatenate((size, jnp.broadcast_to(skip_ref[...], (8, heads))), axis=0)
        row = lax.broadcasted_iota(jnp.int32, (heads, W), 0)
        col = lax.broadcasted_iota(jnp.int32, (heads, W), 1)
        pick = (row == tp * H + col // PD).astype(F32)
        wide = jnp.dot(
            table, pick, preferred_element_type=F32, precision=lax.Precision.HIGHEST)
        row = lax.broadcasted_iota(jnp.int32, (heads, H * S), 0)
        col = lax.broadcasted_iota(jnp.int32, (heads, H * S), 1)
        pick = (row == tp * H + col // S).astype(F32)
        dec_rows[...] = jnp.dot(
            decay, pick, preferred_element_type=F32, precision=lax.Precision.HIGHEST)
        x = channels[0]
        act[0] = wide[:R] * x
        act[1] = channels[1]
        act[2] = channels[2]
        act[3] = wide[R:R + 1] * x
        act[4] = silu(proj_ref[:, :W].astype(F32))

    rows_here = pl.ds(pl.multiple_of(step_id * B, B), B)
    sx, bm, cm, skx, zs = [act[i, rows_here, :] for i in range(5)]
    dec = dec_rows[rows_here, :]
    sxT = jnp.concatenate((sx, jnp.zeros((S - B, W), F32)), axis=0).T
    line = lax.broadcasted_iota(jnp.int32, (B, S), 0)
    hp = S // PD
    gain = gain_ref[:, own_cols]
    for g in range(G):
        y = jnp.zeros((B, S), F32)
        cg = cm[:, g * S:(g + 1) * S].astype(BF16)
        for s in range(B):
            bg = bm[s:s + 1, g * S:(g + 1) * S]
            news = []
            for h in range(g * hp, (g + 1) * hp):
                col = sxT[h * PD:(h + 1) * PD, s:s + 1]
                new = dec[s:s + 1, h * S:(h + 1) * S] * st_ref[s, h] + col * bg
                ns_ref[s, h] = new
                news.append(new.astype(BF16))
            y = jnp.where(line == s, nt(cg, jnp.concatenate(news, axis=0)), y)
        cols = slice(g * S, (g + 1) * S)
        v = (y + skx[:, cols]) * zs[:, cols]
        v = v * lax.rsqrt(jnp.mean(v * v, axis=-1, keepdims=True) + epsilon)
        out_ref[:, cols] = v * gain[:, cols]


def ffn_kernel(
    N, T, mix_ref, res_ref, fgain_ref, routes_ref, rw_ref, blend_ref,
    wo_h, eg_h, eu_h, ed_h, dg_h, du_h, dd_h, out_ref,
    wo, eg, eu, ed, dg, du, dd, rsb, rsin, ag, nfall, wts, outb, pin, qb, inb, ob, opin, fb,
    fin_in, own_acc,
    wsem, sa, ra, sb, rb, sc, rc, sd, rd, sg, rg, sh, rh, se, re_, so, ro, sf, rf,
):
    ep, tp = lax.axis_index("ep"), lax.axis_index("tp")
    R, D = res_ref.shape
    W = D // T
    E = eg_h.shape[0]
    half = R // 2
    core = lax.rem(tp, 2)
    other = 1 - core
    mate = tp + 1 - 2 * core

    def near(o):
        p, bit = 0, 1
        while bit < N:
            p = p + bit * lax.rem(lax.rem(lax.div(ep, bit), 2) + lax.rem(lax.div(o, bit), 2), 2)
            bit *= 2
        return p

    loads = [
        pltpu.make_async_copy(a, b, wsem.at[i])
        for i, (a, b) in enumerate(
            ((wo_h, wo), (dg_h, dg), (du_h, du), (dd_h, dd), (eg_h, eg), (eu_h, eu), (ed_h, ed)))
    ]
    for c in loads:
        c.start()
    bar = pltpu.get_barrier_semaphore()

    def greet_ep(o, _):
        pl.semaphore_signal(bar, inc=1, device_id=(lax.rem(ep + o, N), tp), device_id_type=MESH)
        return 0

    def greet_tp(o, _):
        pl.semaphore_signal(bar, inc=1, device_id=(ep, lax.rem(tp + o, T)), device_id_type=MESH)
        return 0

    lax.fori_loop(1, N, greet_ep, 0)
    lax.fori_loop(1, T, greet_tp, 0)

    L = wts.shape[2]
    line = lax.broadcasted_iota(jnp.int32, (L, R), 0)
    table = jnp.zeros((L, R), F32)
    for k in range(routes_ref.shape[0]):
        table = table + jnp.where(line == routes_ref[k:k + 1, :], rw_ref[k:k + 1, :], 0.0)
    eye = (lax.broadcasted_iota(jnp.int32, (L, L), 0) == lax.broadcasted_iota(jnp.int32, (L, L), 1))
    wts[ep] = lax.dot_general(
        table, eye.astype(F32), (((0,), (0,)), ((), ())), preferred_element_type=F32,
        precision=lax.Precision.HIGHEST)

    loads[0].wait()
    mixed = mix_ref[...].astype(BF16)
    for k in range(T):
        rsb[k] = mm(mixed, wo[:, k * W:(k + 1) * W]).astype(BF16)
    pl.semaphore_wait(bar, N - 1 + T - 1)

    def tp_copy(src, dst, ss, rs, peer):
        return pltpu.make_async_remote_copy(
            src_ref=src, dst_ref=dst, send_sem=ss, recv_sem=rs,
            device_id=(ep, peer), device_id_type=MESH)

    def ep_copy(src, dst, ss, rs, peer):
        return pltpu.make_async_remote_copy(
            src_ref=src, dst_ref=dst, send_sem=ss, recv_sem=rs,
            device_id=(peer, tp), device_id_type=MESH)

    def send_a(o, _):
        p = lax.rem(tp + o, T)
        tp_copy(rsb.at[p], rsin.at[tp], sa.at[p], ra.at[tp], p).start()
        return 0

    lax.fori_loop(1, T, send_a, 0)

    def send_w(o, _):
        p = lax.rem(ep + o, N)
        ep_copy(wts.at[ep], wts.at[ep], sb.at[p], rb.at[ep], p).start()
        return 0

    lax.fori_loop(1, N, send_w, 0)

    def sum_a(o, acc):
        p = lax.rem(tp + o, T)
        tp_copy(rsb.at[p], rsin.at[p], sa.at[p], ra.at[p], p).wait_recv()
        return acc + rsin[p].astype(F32)

    total = lax.fori_loop(1, T, sum_a, rsb[tp].astype(F32))
    own_cols = pl.ds(pl.multiple_of(tp * W, W), W)
    ag[tp] = (res_ref[:, own_cols].astype(F32) + total).astype(BF16)

    def send_c(o, _):
        p = lax.rem(tp + o, T)
        tp_copy(ag.at[tp], ag.at[tp], sc.at[p], rc.at[tp], p).start()
        return 0

    lax.fori_loop(1, T, send_c, 0)

    def wait_c(o, _):
        p = lax.rem(tp + o, T)
        tp_copy(ag.at[p], ag.at[p], sc.at[p], rc.at[p], p).wait_recv()
        return 0

    lax.fori_loop(1, T, wait_c, 0)
    sq = jnp.zeros((R, 1), F32)
    for k in range(T):
        v = ag[k].astype(F32)
        sq = sq + jnp.sum(v * v, axis=-1, keepdims=True)
    scale = lax.rsqrt(sq / D + epsilon)
    for k in range(T):
        cols = slice(k * W, (k + 1) * W)
        v = (ag[k].astype(F32) * scale * fgain_ref[:, cols]).astype(BF16)
        nfall[ep, 0, :, cols] = v[:half]
        nfall[ep, 1, :, cols] = v[half:]

    def send_d(o, _):
        p = near(o)
        ep_copy(nfall.at[ep, core], nfall.at[ep, core], sd.at[p], rd.at[ep], p).start()
        return 0

    lax.fori_loop(1, N, send_d, 0)

    nf = nfall[ep].reshape(R, D)
    for c in loads[1:4]:
        c.wait()
    dh = (silu(mm(nf, dg[...])) * mm(nf, du[...])).astype(BF16)
    blend = jnp.sum(nf.astype(F32) * blend_ref[...].astype(F32).reshape(1, D), axis=-1, keepdims=True)
    mixw = jax.nn.sigmoid(blend)
    own = mm(dh, dd[...]) * mixw
    for c in loads[4:]:
        c.wait()

    elane = lax.broadcasted_iota(jnp.int32, (R, wts.shape[2]), 1)

    def experts(p):
        rows = nfall[p].reshape(R, D)
        table = wts[p]
        acc = None
        for e in range(E):
            coef = jnp.sum(jnp.where(elane == ep * E + e, table, 0.0), axis=-1, keepdims=True)
            h = (silu(mm(rows, eg[e])) * mm(rows, eu[e])).astype(BF16)
            part = mm(h, ed[e]) * coef
            acc = part if acc is None else acc + part
        return acc

    own_acc[...] = (own + experts(ep)).reshape(2, half, D)
    ob[...] = own_acc[other].astype(BF16)
    own_swap = tp_copy(ob, opin, so.at[0], ro.at[0], mate)
    own_swap.start()

    def forward(o, _):
        p = near(o)
        ep_copy(nfall.at[p, core], nfall.at[p, core], sd.at[p], rd.at[p], p).wait_recv()
        tp_copy(nfall.at[p, core], nfall.at[p, core], sg.at[p], rg.at[p], mate).start()
        return 0

    lax.fori_loop(1, N, forward, 0)

    def hand_back(o):
        p = near(o)
        tp_copy(outb.at[p, other], pin.at[p], sh.at[p], rh.at[p], mate).wait_recv()
        qb[p] = (outb[p, core].astype(F32) + pin[p].astype(F32)).astype(BF16)
        ep_copy(qb.at[p], inb.at[ep], se.at[p], re_.at[ep], p).start()

    def visit(o, _):
        p = near(o)
        ep_copy(wts.at[p], wts.at[p], sb.at[p], rb.at[p], p).wait_recv()
        tp_copy(nfall.at[p, other], nfall.at[p, other], sg.at[p], rg.at[p], mate).wait_recv()
        outb[p] = experts(p).astype(BF16).reshape(2, half, D)
        tp_copy(outb.at[p, other], pin.at[p], sh.at[p], rh.at[p], mate).start()

        @pl.when(o > 1)
        def _():
            hand_back(o - 1)

        return 0

    lax.fori_loop(1, N, visit, 0)
    hand_back(jnp.int32(N - 1))
    own_swap.wait()
    own_acc[core] += opin[...].astype(F32)

    def gather_e(o, _):
        p = near(o)
        ep_copy(qb.at[p], inb.at[p], se.at[p], re_.at[p], p).wait_recv()
        own_acc[core] += inb[p].astype(F32)
        return 0

    lax.fori_loop(1, N, gather_e, 0)
    for k in range(T):
        fb[k] = own_acc[core, :, k * W:(k + 1) * W].astype(BF16)

    def send_f(o, _):
        p = lax.rem(tp + o, T)
        tp_copy(fb.at[p], fin_in.at[tp], sf.at[p], rf.at[tp], p).start()
        return 0

    lax.fori_loop(1, T, send_f, 0)
    fin_in[tp] = fb[tp]

    def wait_f(o, _):
        p = lax.rem(tp + o, T)
        tp_copy(fb.at[p], fin_in.at[p], sf.at[p], rf.at[p], p).wait_recv()
        return 0

    lax.fori_loop(1, T, wait_f, 0)
    halves = [sum(fin_in[k].astype(F32) for k in range(i, T, 2)) for i in range(2)]
    final = jnp.concatenate(halves, axis=0) + ag[tp].astype(F32)
    out_ref[...] = final.astype(BF16)

    def done_tp(o, _):
        p = lax.rem(tp + o, T)
        tp_copy(rsb.at[p], rsin.at[p], sa.at[p], ra.at[p], p).wait_send()
        tp_copy(ag.at[tp], ag.at[tp], sc.at[p], rc.at[p], p).wait_send()
        tp_copy(fb.at[p], fin_in.at[p], sf.at[p], rf.at[p], p).wait_send()
        return 0

    def done_ep(o, _):
        p = near(o)
        ep_copy(wts.at[ep], wts.at[ep], sb.at[p], rb.at[p], p).wait_send()
        ep_copy(nfall.at[ep, core], nfall.at[ep, core], sd.at[p], rd.at[p], p).wait_send()
        tp_copy(nfall.at[p, core], nfall.at[p, core], sg.at[p], rg.at[p], mate).wait_send()
        tp_copy(outb.at[p, other], pin.at[p], sh.at[p], rh.at[p], mate).wait_send()
        ep_copy(qb.at[p], inb.at[p], se.at[p], re_.at[p], p).wait_send()
        return 0

    lax.fori_loop(1, T, done_tp, 0)
    lax.fori_loop(1, N, done_ep, 0)


def on_device(
    residual, mixer_gain, gate_proj, input_proj, write_proj, read_proj, step_proj, conv_weight,
    step_bias, log_rate, skip_gain, group_gain, ssm_state, conv_state, out_proj, ffn_gain, routes,
    route_weight, expert_gate, expert_up, expert_down, dense_gate, dense_up, dense_down,
    blend_weight,
):
    N, T = lax.axis_size("ep"), lax.axis_size("tp")
    R, D = residual.shape
    K, W = gate_proj.shape
    H, PD, S = ssm_state.shape[1:]
    E = expert_gate.shape[0]
    heads = step_proj.shape[1]
    dma = pltpu.SemaphoreType.DMA

    projected, step_raw = pl.pallas_call(
        functools.partial(proj_kernel, N),
        out_shape=(jax.ShapeDtypeStruct((R, 4 * W), BF16), jax.ShapeDtypeStruct((R, heads), F32)),
        in_specs=[VM, VM, HB, HB, HB, HB, VM],
        out_specs=(VM, VM),
        scratch_shapes=[
            pltpu.VMEM((4, K, W), BF16), pltpu.VMEM((N, R, K), BF16), pltpu.VMEM((N, R, K), BF16),
            pltpu.VMEM((N, R, 4 * W), BF16), pltpu.VMEM((N, R, 4 * W), BF16),
            dma((4,)), dma((N,)), dma((N,)), dma((N,)), dma((N,)),
        ],
        compiler_params=pltpu.CompilerParams(
            collective_id=0, has_side_effects=True, vmem_limit_bytes=GRANT),
        name="proj",
    )(residual, mixer_gain.reshape(1, D), gate_proj, input_proj, write_proj, read_proj, step_proj.T)

    B = 8
    kept = conv_state.shape[1]
    new_state, conv_out, mixed = pl.pallas_call(
        mixer_kernel,
        grid=(R // B,),
        out_shape=(
            jax.ShapeDtypeStruct(ssm_state.shape, F32),
            jax.ShapeDtypeStruct((kept, 3, R, W), BF16),
            jax.ShapeDtypeStruct((R, W), F32),
        ),
        in_specs=[
            pl.BlockSpec((R, 4 * W), lambda i: (0, 0)),
            pl.BlockSpec((R, heads), lambda i: (0, 0)),
            pl.BlockSpec((1, heads), lambda i: (0, 0)),
            pl.BlockSpec((1, heads), lambda i: (0, 0)),
            pl.BlockSpec((1, heads), lambda i: (0, 0)),
            pl.BlockSpec((1, T * W), lambda i: (0, 0)),
            pl.BlockSpec((3, kept + 1, T * W), lambda i: (0, 0, 0)),
            pl.BlockSpec((kept, 3, R, W), lambda i: (0, 0, 0, 0)),
            pl.BlockSpec((B, H, PD, S), lambda i: (i, 0, 0, 0)),
        ],
        out_specs=(
            pl.BlockSpec((B, H, PD, S), lambda i: (i, 0, 0, 0)),
            pl.BlockSpec((kept, 3, R, W), lambda i: (0, 0, 0, 0)),
            pl.BlockSpec((B, W), lambda i: (i, 0)),
        ),
        scratch_shapes=[pltpu.VMEM((5, R, W), F32), pltpu.VMEM((R, H * S), F32)],
        compiler_params=pltpu.CompilerParams(
            dimension_semantics=("arbitrary",), vmem_limit_bytes=GRANT),
        name="mixer",
    )(projected, step_raw, step_bias.reshape(1, heads), log_rate.reshape(1, heads),
      skip_gain.reshape(1, heads), group_gain.reshape(1, T * W),
      conv_weight.transpose(1, 0, 2), conv_state.transpose(1, 2, 0, 3), ssm_state)
    new_conv = conv_out.transpose(2, 0, 1, 3)

    lanes = max(128, -(-E * N // 128) * 128)
    layer_out = pl.pallas_call(
        functools.partial(ffn_kernel, N, T),
        out_shape=jax.ShapeDtypeStruct((R, W), BF16),
        in_specs=[VM] * 6 + [HB] * 7,
        out_specs=VM,
        scratch_shapes=[
            pltpu.VMEM((W, D), BF16), pltpu.VMEM((E, D, W), BF16), pltpu.VMEM((E, D, W), BF16),
            pltpu.VMEM((E, W, D), BF16), pltpu.VMEM((D, W), BF16), pltpu.VMEM((D, W), BF16),
            pltpu.VMEM((W, D), BF16),
            pltpu.VMEM((T, R, W), BF16), pltpu.VMEM((T, R, W), BF16), pltpu.VMEM((T, R, W), BF16),
            pltpu.VMEM((N, 2, R // 2, D), BF16), pltpu.VMEM((N, R, lanes), F32),
            pltpu.VMEM((N, 2, R // 2, D), BF16), pltpu.VMEM((N, R // 2, D), BF16),
            pltpu.VMEM((N, R // 2, D), BF16), pltpu.VMEM((N, R // 2, D), BF16),
            pltpu.VMEM((R // 2, D), BF16), pltpu.VMEM((R // 2, D), BF16),
            pltpu.VMEM((T, R // 2, W), BF16), pltpu.VMEM((T, R // 2, W), BF16),
            pltpu.VMEM((2, R // 2, D), F32),
            dma((7,)), dma((T,)), dma((T,)), dma((N,)), dma((N,)), dma((T,)), dma((T,)),
            dma((N,)), dma((N,)), dma((N,)), dma((N,)), dma((N,)), dma((N,)), dma((N,)), dma((N,)),
            dma((1,)), dma((1,)), dma((T,)), dma((T,)),
        ],
        compiler_params=pltpu.CompilerParams(
            collective_id=1, has_side_effects=True, vmem_limit_bytes=GRANT),
        name="ffn",
    )(mixed, residual, ffn_gain.reshape(1, D), routes.T, route_weight.T, blend_weight,
      out_proj, expert_gate, expert_up, expert_down, dense_gate, dense_up, dense_down)
    return (layer_out, new_state, new_conv)


def solution(mesh):
    return jax.shard_map(
        on_device,
        mesh=mesh,
        in_specs=(
            P("ep", None), P(), P("ep", "tp"), P("ep", "tp"), P("ep", "tp"), P("ep", "tp"),
            P(), P(), P(), P(), P(), P(),
            P("ep", "tp", None, None), P("ep", None, None, "tp"), P("tp", None), P(),
            P("ep", None), P("ep", None), P("ep", None, "tp"), P("ep", None, "tp"),
            P("ep", "tp", None), P(None, "tp"), P(None, "tp"), P("tp", None), P(),
        ),
        out_specs=(P("ep", "tp"), P("ep", "tp", None, None), P("ep", None, None, "tp")),
        check_vma=False,
    )
```

profile of v0, /device:TPU:0, one launch (start us, length us, event | category | flops | bytes accessed | tf_op | source)
XLA Modules:
  0.0 54.9 jit_solution(12008925658017650055)
XLA Ops:
  0.6 13.5 %proj.1 = (bf16[32,1024]{1,0:T(8,128)(2,1)}, f32[32,32]{1,0:T(8,128)}) custom-call(bf16[32,2048]{1,0:T(8,128)(2,1)} %res_ref.3, f32[1,2048]{1,0:T(1,128)} %bitcast.15, bf16[512,256]{1,0:T(8,128)(2,1)} %wg.1, bf16[512,256]{1,0:T(8,128)(2,1)} %wx.1, bf16[512,256]{1,0:T(8,128)(2,1)} %wb.1, bf16[512,256]{1,0:T(8,128)(2,1)} %wc.1, bf16[32,2048]{1,0:T(8,128)(2,1)} %bitcast.13), custom_call_target="tpu_custom_call" | custom-call | tf_op jit(solution)/shard_map/proj/pallas_call | solution.py:419
  14.1 6.3 %mixer.1 = (f32[32,4,64,128]{3,2,1,0:T(8,128)}, bf16[3,3,32,256]{3,2,1,0:T(8,128)(2,1)}, f32[32,256]{1,0:T(8,128)}) custom-call(bf16[32,1024]{1,0:T(8,128)(2,1)} %get-tuple-element.8.proj_ref, f32[32,32]{1,0:T(8,128)} %get-tuple-element.9.raw_ref, f32[1,32]{1,0:T(1,128)} %bitcast.20, f32[1,32]{1,0:T(1,128)} %bitcast.21, f32[1,32]{1,0:T(1,128)} %bitcast.22, ...), custom_call_target="tpu_custom_call" | custom-call | tf_op jit(solution)/shard_map/mixer/pallas_call | solution.py:436
  20.4 33.2 %ffn.1 = bf16[32,256]{1,0:T(8,128)(2,1)} custom-call(f32[32,256]{1,0:T(8,128)} %get-tuple-element.10.mix_ref, bf16[32,2048]{1,0:T(8,128)(2,1)} %res_ref.3, f32[1,2048]{1,0:T(1,128)} %bitcast.17, s32[2,32]{1,0:T(2,128)} %bitcast.18, f32[2,32]{1,0:T(2,128)} %bitcast.19, bf16[2048]{0:T(1024)(128)(2,1)} %blend_ref.1, bf16[256,2048]{1,0:T(8,128)(2,1)} %wo_h.1, ...), custom_call_target="tpu_custom_call" | custom-call | tf_op jit(solution)/shard_map/ffn/pallas_call | solution.py:470
  53.6 1.3 %copy.29 = bf16[32,256]{1,0:T(8,128)(2,1)} copy(bf16[32,256]{1,0:T(8,128)(2,1)} %ffn.1) | data formatting | bytes 32768
where the time goes:
time: 55.2 us; the launch traced here: 54.9 us
  Pallas kernels  52.9 us (96%)
  local copies, waits for them, and re-layouts  1.32 us (2%)
  between operations  0.65 us (1%)
    pallas_call x1, Pallas kernels, on_device(): pl.pallas_call(functools.partial(ffn_kernel, N, T), out_shape=jax.ShapeDt...  33.2 us
    pallas_call x1, Pallas kernels, on_device(): pl.pallas_call(functools.partial(proj_kernel, N), out_shape=(jax.ShapeDty...  13.5 us
    pallas_call x1, Pallas kernels, on_device(): pl.pallas_call(mixer_kernel, grid=(R // B,), out_shape=(jax.ShapeDtypeStr...  6.32 us
    unnamed x1, local copies, waits for them, and re-layouts  1.32 us

commit v1 on v0

v1 whole, which is shorter than its diff:
```python
import functools
import jax
import jax.numpy as jnp
from jax import lax
from jax.experimental import pallas as pl
from jax.experimental.pallas import tpu as pltpu
from jax.sharding import PartitionSpec as P

epsilon = 1e-06
F32 = jnp.float32
BF16 = jnp.bfloat16
MESH = pl.DeviceIdType.MESH
VM = pl.BlockSpec(memory_space=pltpu.VMEM)
HB = pl.BlockSpec(memory_space=pltpu.HBM)
GRANT = 50 * 2**20
GRANT2 = 8 * 2**20


def mm(a, b):
    return jnp.dot(a, b, preferred_element_type=F32)


def nt(a, b):
    return lax.dot_general(a, b, (((1,), (1,)), ((), ())), preferred_element_type=F32)


def silu(v):
    return v * jax.nn.sigmoid(v)


def layer_kernel(
    N, T, res_h, mgain_h, wg_h, wx_h, wb_h, wc_h, step_h, bias_h, rate_h, skip_h, ggain_h, taps_h,
    conv_h, st_h, fgain_h, routes_h, rw_h, blend_h, wo_h, eg_h, eu_h, ed_h, dg_h, du_h, dd_h,
    ns_ref, nc_ref, out_ref,
    res, mgain, w, stepw, bias, rate, skip, ggain, taps, conv, st, fgain, routes, rw, blend,
    wo, eg, eu, ed, dg, du, dd,
    nb, pieces, outb1, inb1, s16, dec_rows, act,
    rsb, rsin, ag, nfall, wts, outb, pin, qb, inb, ob, opin, fb, fin_in, own_acc,
    lsem, s1, r1, s2, r2,
    sa, ra, sb, rb, sc, rc, sd, rd, sg, rg, sh, rh, se, re_, so, ro, sf, rf,
):
    ep, tp = lax.axis_index("ep"), lax.axis_index("tp")
    R, D = res.shape
    K = D // N
    W = D // T
    E = eg.shape[0]
    H, PD, S = st.shape[1:]
    G = W // S
    hp = S // PD
    heads = stepw.shape[0]
    kept = conv.shape[0]
    half = R // 2
    core = lax.rem(tp, 2)
    other = 1 - core
    mate = tp + 1 - 2 * core
    own_cols = pl.ds(pl.multiple_of(tp * W, W), W)

    def near(o):
        p, bit = 0, 1
        while bit < N:
            p = p + bit * lax.rem(lax.rem(lax.div(ep, bit), 2) + lax.rem(lax.div(o, bit), 2), 2)
            bit *= 2
        return p

    def tp_copy(src, dst, ss, rs, peer):
        return pltpu.make_async_remote_copy(
            src_ref=src, dst_ref=dst, send_sem=ss, recv_sem=rs,
            device_id=(ep, peer), device_id_type=MESH)

    def ep_copy(src, dst, ss, rs, peer):
        return pltpu.make_async_remote_copy(
            src_ref=src, dst_ref=dst, send_sem=ss, recv_sem=rs,
            device_id=(peer, tp), device_id_type=MESH)

    sources = (
        (res_h, res), (mgain_h, mgain), (wg_h, w.at[0]), (wx_h, w.at[1]), (wb_h, w.at[2]),
        (wc_h, w.at[3]), (step_h, stepw), (bias_h, bias), (rate_h, rate), (skip_h, skip),
        (routes_h, routes), (rw_h, rw), (st_h, st), (conv_h, conv), (taps_h.at[:, :, own_cols], taps),
        (ggain_h.at[:, own_cols], ggain), (wo_h, wo), (fgain_h, fgain), (blend_h, blend),
        (dg_h, dg), (du_h, du), (dd_h, dd), (eg_h, eg), (eu_h, eu), (ed_h, ed),
    )
    loads = [pltpu.make_async_copy(a, b, lsem.at[i]) for i, (a, b) in enumerate(sources)]
    bar = pltpu.get_barrier_semaphore()

    def greet_ep(o, _):
        pl.semaphore_signal(bar, inc=1, device_id=(lax.rem(ep + o, N), tp), device_id_type=MESH)
        return 0

    def greet_tp(o, _):
        pl.semaphore_signal(bar, inc=1, device_id=(ep, lax.rem(tp + o, T)), device_id_type=MESH)
        return 0

    for c in loads[:2]:
        c.start()
    lax.fori_loop(1, N, greet_ep, 0)
    lax.fori_loop(1, T, greet_tp, 0)
    for c in loads[2:12]:
        c.start()
    for c in loads[:2]:
        c.wait()
    x = res[...].astype(F32)
    normed = x * lax.rsqrt(jnp.mean(x * x, axis=-1, keepdims=True) + epsilon) * mgain[...]
    normed = normed.astype(BF16)
    for k in range(N):
        nb[k] = normed[:, k * K:(k + 1) * K]
    pl.semaphore_wait(bar, N - 1 + T - 1)

    def send1(o, _):
        p = near(o)
        ep_copy(nb.at[p], pieces.at[ep], s1.at[p], r1.at[ep], p).start()
        return 0

    lax.fori_loop(1, N, send1, 0)
    for c in loads[12:17]:
        c.start()
    for c in loads[6:12]:
        c.wait()

    raw = nt(normed, stepw[...])
    size = jax.nn.softplus(raw + bias[...])
    decay = jnp.exp(-jnp.exp(rate[...]) * size)
    table = jnp.concatenate((size, decay, jnp.broadcast_to(skip[...], (8, heads))), axis=0)
    row = lax.broadcasted_iota(jnp.int32, (heads, W), 0)
    col = lax.broadcasted_iota(jnp.int32, (heads, W), 1)
    pick = (row == tp * H + col // PD).astype(F32)
    wide = jnp.dot(table, pick, preferred_element_type=F32, precision=lax.Precision.HIGHEST)
    row = lax.broadcasted_iota(jnp.int32, (heads, H * S), 0)
    col = lax.broadcasted_iota(jnp.int32, (heads, H * S), 1)
    pick = (row == tp * H + col // S).astype(F32)
    dec_rows[...] = jnp.dot(decay, pick, preferred_element_type=F32, precision=lax.Precision.HIGHEST)

    L = wts.shape[2]
    line = lax.broadcasted_iota(jnp.int32, (L, R), 0)
    table = jnp.zeros((L, R), F32)
    for k in range(routes.shape[0]):
        table = table + jnp.where(line == routes[k:k + 1, :], rw[k:k + 1, :], 0.0)
    eye = (lax.broadcasted_iota(jnp.int32, (L, L), 0) == lax.broadcasted_iota(jnp.int32, (L, L), 1))
    wts[ep] = lax.dot_general(
        table, eye.astype(F32), (((0,), (0,)), ((), ())), preferred_element_type=F32,
        precision=lax.Precision.HIGHEST)

    for c in loads[2:6]:
        c.wait()
    own = [mm(nb[ep], w[i]) for i in range(4)]

    def step(o, _):
        p = near(o)
        ep_copy(nb.at[p], pieces.at[p], s1.at[p], r1.at[p], p).wait_recv()
        a = pieces[p]
        for i in range(4):
            outb1[p, :, i * W:(i + 1) * W] = mm(a, w[i]).astype(BF16)
        ep_copy(outb1.at[p], inb1.at[ep], s2.at[p], r2.at[ep], p).start()
        return 0

    lax.fori_loop(1, N, step, 0)

    def send_w(o, _):
        p = near(o)
        ep_copy(wts.at[ep], wts.at[ep], sb.at[p], rb.at[ep], p).start()
        return 0

    lax.fori_loop(1, N, send_w, 0)
    for c in loads[17:]:
        c.start()
    for c in loads[12:16]:
        c.wait()

    def narrow(i, _):
        for j in range(4):
            s = i * 4 + j
            for g in range(G):
                s16[s, :, g * S:(g + 1) * S] = st[s, g * hp:(g + 1) * hp].reshape(S, S).astype(BF16)
        return 0

    lax.fori_loop(0, R // 4, narrow, 0)
    for c in range(3):
        part = jnp.zeros((R, W), F32)
        for k in range(kept):
            part = part + conv[k, c].astype(F32) * taps[c, k:k + 1, :]
        act[c] = part
        for k in range(kept - 1):
            nc_ref[k, c] = conv[k + 1, c]

    total = jnp.concatenate(own, axis=1)
    for o in range(1, N):
        p = near(o)
        ep_copy(outb1.at[p], inb1.at[p], s2.at[p], r2.at[p], p).wait_recv()
        total = total + inb1[p].astype(F32)
    proj = total.astype(BF16)
    channels = []
    for c in range(3):
        newest = proj[:, (c + 1) * W:(c + 2) * W]
        nc_ref[kept - 1, c] = newest
        channels.append(silu(act[c] + newest.astype(F32) * taps[c, kept:kept + 1, :]))
    xa, bm, cm = channels
    sx = wide[:R] * xa
    act[0] = sx
    act[1] = bm
    lane = lax.broadcasted_iota(jnp.int32, (8, W), 1) // S
    line = lax.broadcasted_iota(jnp.int32, (8, S), 0)
    rows_out = []
    for blk in range(R // 8):
        c8 = cm[blk * 8:(blk + 1) * 8]
        lhs = jnp.concatenate([jnp.where(lane == g, c8, 0.0) for g in range(G)], axis=0).astype(BF16)
        ys = [jnp.zeros((8, S), F32) for _ in range(G)]
        for j in range(0, 8, 2):
            s = blk * 8 + j
            got = nt(lhs, s16[s:s + 2].reshape(2 * S, W))
            for g in range(G):
                for i in range(2):
                    ys[g] = jnp.where(line == j + i, got[g * 8:(g + 1) * 8, i * S:(i + 1) * S], ys[g])
        rows_out.append(jnp.concatenate(ys, axis=1))
    y = wide[R:2 * R] * jnp.concatenate(rows_out, axis=0)
    bc = bm * cm
    z = silu(proj[:, :W].astype(F32))
    direct = wide[2 * R:2 * R + 1] * xa
    mixed = []
    for g in range(G):
        cols = slice(g * S, (g + 1) * S)
        dots = jnp.sum(bc[:, cols], axis=-1, keepdims=True)
        v = (y[:, cols] + dots * sx[:, cols] + direct[:, cols]) * z[:, cols]
        v = v * lax.rsqrt(jnp.mean(v * v, axis=-1, keepdims=True) + epsilon)
        mixed.append((v * ggain[:, cols]).astype(BF16))
    mixed = jnp.concatenate(mixed, axis=1)
    loads[16].wait()
    for k in range(T):
        rsb[k] = mm(mixed, wo[:, k * W:(k + 1) * W]).astype(BF16)

    def send_a(o, _):
        p = lax.rem(tp + o, T)
        tp_copy(rsb.at[p], rsin.at[tp], sa.at[p], ra.at[tp], p).start()
        return 0

    lax.fori_loop(1, T, send_a, 0)

    def update(i, _):
        here = pl.ds(pl.multiple_of(i * 8, 8), 8)
        sx8, b8, dec = act[0, here, :], act[1, here, :], dec_rows[here, :]
        sxT = jnp.concatenate((sx8, jnp.zeros((S - 8, W), F32)), axis=0).T
        for g in range(G):
            for j in range(8):
                bg = b8[j:j + 1, g * S:(g + 1) * S]
                for h in range(g * hp, (g + 1) * hp):
                    column = sxT[h * PD:(h + 1) * PD, j:j + 1]
                    ns_ref[i * 8 + j, h] = dec[j:j + 1, h * S:(h + 1) * S] * st[i * 8 + j, h] + column * bg
        return 0

    lax.fori_loop(0, R // 8, update, 0)

    def sum_a(o, acc):
        p = lax.rem(tp + o, T)
        tp_copy(rsb.at[p], rsin.at[p], sa.at[p], ra.at[p], p).wait_recv()
        return acc + rsin[p].astype(F32)

    total = lax.fori_loop(1, T, sum_a, rsb[tp].astype(F32))
    ag[tp] = (res[:, own_cols].astype(F32) + total).astype(BF16)

    def send_c(o, _):
        p = lax.rem(tp + o, T)
        tp_copy(ag.at[tp], ag.at[tp], sc.at[p], rc.at[tp], p).start()
        return 0

    lax.fori_loop(1, T, send_c, 0)

    def wait_c(o, _):
        p = lax.rem(tp + o, T)
        tp_copy(ag.at[p], ag.at[p], sc.at[p], rc.at[p], p).wait_recv()
        return 0

    lax.fori_loop(1, T, wait_c, 0)
    loads[17].wait()
    sq = jnp.zeros((R, 1), F32)
    for k in range(T):
        v = ag[k].astype(F32)
        sq = sq + jnp.sum(v * v, axis=-1, keepdims=True)
    scale = lax.rsqrt(sq / D + epsilon)
    for k in range(T):
        cols = slice(k * W, (k + 1) * W)
        v = (ag[k].astype(F32) * scale * fgain[:, cols]).astype(BF16)
        nfall[ep, 0, :, cols] = v[:half]
        nfall[ep, 1, :, cols] = v[half:]

    def send_d(o, _):
        p = near(o)
        ep_copy(nfall.at[ep, core], nfall.at[ep, core], sd.at[p], rd.at[ep], p).start()
        return 0

    lax.fori_loop(1, N, send_d, 0)

    nf = nfall[ep].reshape(R, D)
    for c in loads[18:22]:
        c.wait()
    dh = (silu(mm(nf, dg[...])) * mm(nf, du[...])).astype(BF16)
    blend = jnp.sum(nf.astype(F32) * blend[...].astype(F32).reshape(1, D), axis=-1, keepdims=True)
    mixw = jax.nn.sigmoid(blend)
    own = mm(dh, dd[...]) * mixw
    for c in loads[22:]:
        c.wait()

    elane = lax.broadcasted_iota(jnp.int32, (R, wts.shape[2]), 1)

    def experts(p):
        rows = nfall[p].reshape(R, D)
        table = wts[p]
        acc = None
        for e in range(E):
            coef = jnp.sum(jnp.where(elane == ep * E + e, table, 0.0), axis=-1, keepdims=True)
            h = (silu(mm(rows, eg[e])) * mm(rows, eu[e])).astype(BF16)
            part = mm(h, ed[e]) * coef
            acc = part if acc is None else acc + part
        return acc

    own_acc[...] = (own + experts(ep)).reshape(2, half, D)
    ob[...] = own_acc[other].astype(BF16)
    own_swap = tp_copy(ob, opin, so.at[0], ro.at[0], mate)
    own_swap.start()

    def forward(o, _):
        p = near(o)
        ep_copy(nfall.at[p, core], nfall.at[p, core], sd.at[p], rd.at[p], p).wait_recv()
        tp_copy(nfall.at[p, core], nfall.at[p, core], sg.at[p], rg.at[p], mate).start()
        return 0

    lax.fori_loop(1, N, forward, 0)

    def hand_back(o):
        p = near(o)
        tp_copy(outb.at[p, other], pin.at[p], sh.at[p], rh.at[p], mate).wait_recv()
        qb[p] = (outb[p, core].astype(F32) + pin[p].astype(F32)).astype(BF16)
        ep_copy(qb.at[p], inb.at[ep], se.at[p], re_.at[ep], p).start()

    def visit(o, _):
        p = near(o)
        ep_copy(wts.at[p], wts.at[p], sb.at[p], rb.at[p], p).wait_recv()
        tp_copy(nfall.at[p, other], nfall.at[p, other], sg.at[p], rg.at[p], mate).wait_recv()
        outb[p] = experts(p).astype(BF16).reshape(2, half, D)
        tp_copy(outb.at[p, other], pin.at[p], sh.at[p], rh.at[p], mate).start()

        @pl.when(o > 1)
        def _():
            hand_back(o - 1)

        return 0

    lax.fori_loop(1, N, visit, 0)
    hand_back(jnp.int32(N - 1))
    own_swap.wait()
    own_acc[core] += opin[...].astype(F32)

    def gather_e(o, _):
        p = near(o)
        ep_copy(qb.at[p], inb.at[p], se.at[p], re_.at[p], p).wait_recv()
        own_acc[core] += inb[p].astype(F32)
        return 0

    lax.fori_loop(1, N, gather_e, 0)
    for k in range(T):
        fb[k] = own_acc[core, :, k * W:(k + 1) * W].astype(BF16)

    def send_f(o, _):
        p = lax.rem(tp + o, T)
        tp_copy(fb.at[p], fin_in.at[tp], sf.at[p], rf.at[tp], p).start()
        return 0

    lax.fori_loop(1, T, send_f, 0)
    fin_in[tp] = fb[tp]

    def wait_f(o, _):
        p = lax.rem(tp + o, T)
        tp_copy(fb.at[p], fin_in.at[p], sf.at[p], rf.at[p], p).wait_recv()
        return 0

    lax.fori_loop(1, T, wait_f, 0)
    halves = [sum(fin_in[k].astype(F32) for k in range(i, T, 2)) for i in range(2)]
    final = jnp.concatenate(halves, axis=0) + ag[tp].astype(F32)
    out_ref[...] = final.astype(BF16)

    def done_tp(o, _):
        p = lax.rem(tp + o, T)
        tp_copy(rsb.at[p], rsin.at[p], sa.at[p], ra.at[p], p).wait_send()
        tp_copy(ag.at[tp], ag.at[tp], sc.at[p], rc.at[p], p).wait_send()
        tp_copy(fb.at[p], fin_in.at[p], sf.at[p], rf.at[p], p).wait_send()
        return 0

    def done_ep(o, _):
        p = near(o)
        ep_copy(nb.at[p], pieces.at[p], s1.at[p], r1.at[p], p).wait_send()
        ep_copy(outb1.at[p], inb1.at[p], s2.at[p], r2.at[p], p).wait_send()
        ep_copy(wts.at[ep], wts.at[ep], sb.at[p], rb.at[p], p).wait_send()
        ep_copy(nfall.at[ep, core], nfall.at[ep, core], sd.at[p], rd.at[p], p).wait_send()
        tp_copy(nfall.at[p, core], nfall.at[p, core], sg.at[p], rg.at[p], mate).wait_send()
        tp_copy(outb.at[p, other], pin.at[p], sh.at[p], rh.at[p], mate).wait_send()
        ep_copy(qb.at[p], inb.at[p], se.at[p], re_.at[p], p).wait_send()
        return 0

    lax.fori_loop(1, T, done_tp, 0)
    lax.fori_loop(1, N, done_ep, 0)


def write_kernel(ns, nc, out, ns_h, nc_h, out_h, sem):
    n = sem.shape[0] - 2
    rows = ns.shape[0] // n
    copies = [
        pltpu.make_async_copy(ns.at[pl.ds(i * rows, rows)], ns_h.at[pl.ds(i * rows, rows)], sem.at[i])
        for i in range(n)
    ]
    copies.append(pltpu.make_async_copy(nc, nc_h, sem.at[n]))
    copies.append(pltpu.make_async_copy(out, out_h, sem.at[n + 1]))
    for c in copies:
        c.start()
    for c in copies:
        c.wait()


def on_device(
    residual, mixer_gain, gate_proj, input_proj, write_proj, read_proj, step_proj, conv_weight,
    step_bias, log_rate, skip_gain, group_gain, ssm_state, conv_state, out_proj, ffn_gain, routes,
    route_weight, expert_gate, expert_up, expert_down, dense_gate, dense_up, dense_down,
    blend_weight,
):
    N, T = lax.axis_size("ep"), lax.axis_size("tp")
    R, D = residual.shape
    K, W = gate_proj.shape
    H, PD, S = ssm_state.shape[1:]
    E = expert_gate.shape[0]
    heads = step_proj.shape[1]
    kept = conv_state.shape[1]
    top = routes.shape[1]
    G = W // S
    dma = pltpu.SemaphoreType.DMA
    V = pltpu.VMEM
    lanes = max(128, -(-E * N // 128) * 128)
    n_in = 25
    new_state, conv_out, last = pl.pallas_call(
        functools.partial(layer_kernel, N, T),
        out_shape=(V(ssm_state.shape, F32), V((kept, 3, R, W), BF16), V((R, W), BF16)),
        in_specs=[HB] * n_in,
        out_specs=(VM, VM, VM),
        scratch_shapes=[
            V((R, D), BF16), V((1, D), F32), V((4, K, W), BF16), V((heads, D), BF16),
            V((1, heads), F32), V((1, heads), F32), V((1, heads), F32), V((1, W), F32),
            V((3, kept + 1, W), F32), V((kept, 3, R, W), BF16), V(ssm_state.shape, F32),
            V((1, D), F32), V((top, R), jnp.int32), V((top, R), F32), V((D,), BF16),
            V((W, D), BF16), V((E, D, W), BF16), V((E, D, W), BF16), V((E, W, D), BF16),
            V((D, W), BF16), V((D, W), BF16), V((W, D), BF16),
            V((N, R, K), BF16), V((N, R, K), BF16), V((N, R, 4 * W), BF16), V((N, R, 4 * W), BF16),
            V((R, S, W), BF16), V((R, H * S), F32), V((3, R, W), F32),
            V((T, R, W), BF16), V((T, R, W), BF16), V((T, R, W), BF16),
            V((N, 2, R // 2, D), BF16), V((N, R, lanes), F32),
            V((N, 2, R // 2, D), BF16), V((N, R // 2, D), BF16),
            V((N, R // 2, D), BF16), V((N, R // 2, D), BF16),
            V((R // 2, D), BF16), V((R // 2, D), BF16),
            V((T, R // 2, W), BF16), V((T, R // 2, W), BF16),
            V((2, R // 2, D), F32),
            dma((n_in,)), dma((N,)), dma((N,)), dma((N,)), dma((N,)),
            dma((T,)), dma((T,)), dma((N,)), dma((N,)), dma((T,)), dma((T,)),
            dma((N,)), dma((N,)), dma((N,)), dma((N,)), dma((N,)), dma((N,)), dma((N,)), dma((N,)),
            dma((1,)), dma((1,)), dma((T,)), dma((T,)),
        ],
        compiler_params=pltpu.CompilerParams(
            collective_id=0, has_side_effects=True, vmem_limit_bytes=GRANT),
        name="layer",
    )(residual, mixer_gain.reshape(1, D), gate_proj, input_proj, write_proj, read_proj, step_proj.T,
      step_bias.reshape(1, heads), log_rate.reshape(1, heads), skip_gain.reshape(1, heads),
      group_gain.reshape(1, D), conv_weight.transpose(1, 0, 2), conv_state.transpose(1, 2, 0, 3),
      ssm_state, ffn_gain.reshape(1, D), routes.T, route_weight.T, blend_weight,
      out_proj, expert_gate, expert_up, expert_down, dense_gate, dense_up, dense_down)
    new_state, conv_out, layer_out = pl.pallas_call(
        write_kernel,
        out_shape=(
            jax.ShapeDtypeStruct(ssm_state.shape, F32),
            jax.ShapeDtypeStruct((kept, 3, R, W), BF16),
            jax.ShapeDtypeStruct((R, W), BF16),
        ),
        in_specs=[VM] * 3,
        out_specs=(HB, HB, HB),
        scratch_shapes=[dma((10,))],
        compiler_params=pltpu.CompilerParams(vmem_limit_bytes=GRANT2),
        name="write",
    )(new_state, conv_out, last)
    return (layer_out, new_state, conv_out.transpose(2, 0, 1, 3))


def solution(mesh):
    return jax.shard_map(
        on_device,
        mesh=mesh,
        in_specs=(
            P("ep", None), P(), P("ep", "tp"), P("ep", "tp"), P("ep", "tp"), P("ep", "tp"),
            P(), P(), P(), P(), P(), P(),
            P("ep", "tp", None, None), P("ep", None, None, "tp"), P("tp", None), P(),
            P("ep", None), P("ep", None), P("ep", None, "tp"), P("ep", None, "tp"),
            P("ep", "tp", None), P(None, "tp"), P(None, "tp"), P("tp", None), P(),
        ),
        out_specs=(P("ep", "tp"), P("ep", "tp", None, None), P("ep", None, None, "tp")),
        check_vma=False,
    )
```

time: 55.2 us -> 45.7 us (0.83)
  Pallas kernels: 52.9 us -> 44.9 us
  local copies, waits for them, and re-layouts: 1.32 us -> 0 us
    pallas_call x3 -> x2, Pallas kernels: 52.9 us -> 44.9 us  [the longest x1 42.8 us: on_device(): pl.pallas_call(functools.partial(layer_kernel, N, T), out_shape=(V(ssm_st...]
    unnamed x1 -> x0, local copies, waits for them, and re-layouts: 1.32 us -> none
where the time goes in v1:
time: 45.7 us; the launch traced here: 45.6 us
  Pallas kernels  44.9 us (98%)
  between operations  0.65 us (1%)
    pallas_call x1, Pallas kernels, on_device(): pl.pallas_call(functools.partial(layer_kernel, N, T), out_shape=(V(ssm_st...  42.8 us
    pallas_call x1, Pallas kernels, on_device(): pl.pallas_call(write_kernel, out_shape=(jax.ShapeDtypeStruct(ssm_state.sh...  2.13 us

profile of v1, /device:TPU:0, one launch (start us, length us, event | category | flops | bytes accessed | tf_op | source)
XLA Modules:
  0.0 45.6 jit_solution(17780585815376302272)
XLA Ops:
  0.6 42.8 %layer.1 = (f32[32,4,64,128]{3,2,1,0:T(8,128)S(1)}, bf16[3,3,32,256]{3,2,1,0:T(8,128)(2,1)S(1)}, bf16[32,256]{1,0:T(8,128)(2,1)S(1)}) custom-call(bf16[32,2048]{1,0:T(8,128)(2,1)} %res_h.1, f32[1,2048]{1,0:T(1,128)} %bitcast.15, bf16[512,256]{1,0:T(8,128)(2,1)} %wg_h.1, bf16[512,256]{1,0:T(8,128)(2,1)} %wx_h.1, bf16[512,256]{1,0:T(8,128)(2,1)} %wb_h.1, ...), custom_call_target="tpu_custom_call" | custom-call | tf_op jit(solution)/shard_map/layer/pallas_call | solution.py:434
  43.4 2.1 %write.1 = (f32[32,4,64,128]{3,2,1,0:T(8,128)}, bf16[3,3,32,256]{3,2,1,0:T(8,128)(2,1)}, bf16[32,256]{1,0:T(8,128)(2,1)}) custom-call(f32[32,4,64,128]{3,2,1,0:T(8,128)S(1)} %get-tuple-element.9.ns, bf16[3,3,32,256]{3,2,1,0:T(8,128)(2,1)S(1)} %get-tuple-element.10.nc, bf16[32,256]{1,0:T(8,128)(2,1)S(1)} %get-tuple-element.11.out), custom_call_target="tpu_custom_call" | custom-call | tf_op jit(solution)/shard_map/write/pallas_call | solution.py:468
